TPU v7x, 512 devices: a whole 4x4x16 slice. The times are simulated.
512 devices in a mesh: sp: 16 (over z), fs: 4 (over y), tp: 8 (over x, core).
Axes of the slice: x: 4, y: 4, z: 16, core: 2. Of those that a mesh axis runs over, the one named last changes fastest.
Arguments:
- input_layer_rows: bfloat16 [4, 4096, 2048], P('fs', 'sp'), may hold values from -6 to 6
- input_norm_gain: float32 [2048], replicated, may hold values from 0.1 to 1.9
- query_weight_attention: bfloat16 [2048, 1024], P(('sp', 'fs'), 'tp'), may hold values from -0.125 to 0.125
- key_weight_attention: bfloat16 [2048, 1024], P(('sp', 'fs'), 'tp'), may hold values from -0.125 to 0.125
- value_weight_attention: bfloat16 [2048, 1024], P(('sp', 'fs'), 'tp'), may hold values from -0.125 to 0.125
- query_weight_recurrent: bfloat16 [2048, 1024], P(('sp', 'fs'), 'tp'), may hold values from -0.125 to 0.125
- forget_weight_recurrent: bfloat16 [2048, 1024], P(('sp', 'fs'), 'tp'), may hold values from -0.125 to 0.125
- value_weight_recurrent: bfloat16 [2048, 1024], P(('sp', 'fs'), 'tp'), may hold values from -0.125 to 0.125
- gate_weight_recurrent: bfloat16 [2048, 1024], P(('sp', 'fs'), 'tp'), may hold values from -0.125 to 0.125
- output_weight_attention: bfloat16 [2048, 1024], P(('sp', 'fs'), 'tp'), may hold values from -0.125 to 0.125
- emitted_projection_linear_scan: bfloat16 [2048, 1024], P(('sp', 'fs'), 'tp'), may hold values from -0.125 to 0.125
- score_offset: float32 [8], P('tp'), as said below
- attention_norm_gain: float32 [1024], P('tp'), may hold values from 0.1 to 1.9
- recurrence_norm_gain: float32 [1024], P('tp'), may hold values from 0.1 to 1.9
- forget_floor: float32 [1024], P('tp'), may hold values from 0.1 to 0.5
- forget_offset: float32 [1024], P('tp'), as said below
- extra_log_decay: float32 [4, 4096, 1024], P('fs', 'sp', 'tp')
Outputs:
- layer_out: bfloat16 [4, 4096, 2048], P('fs', ('sp', 'tp'))
- row_log_total: float32 [4, 8, 4096], P('fs', 'tp', 'sp')
Inputs may be any that keep to these rules, and one draw needn't show every extreme that they name: `score_offset`: each head's offset lies between -ln(4096) - 2 and -ln(4096) + 0.5. `forget_offset`: each channel's offset lies between ln(256) - 3 and ln(4096) + 0.6.
All inputs are finite; a program needn't handle non-finite values.
Results may differ from a plain program's by a relative error of at most 0.015.
Values may be sent and summed in bfloat16 or wider, within the bound.
A program may use at most 64 MiB of HBM per device.

v0:
```python
import jax
import jax.numpy as jnp
from jax import lax
from jax.sharding import PartitionSpec as P

HEAD = 128
BLOCK = 64


epsilon = 1e-06
log_floor = 0.05


def sent_together(arrays, axis, dim, along):
    ends, at = ([], 0)
    for a in arrays[:-1]:
        at += a.shape[along]
        ends.append(at)
    both = jnp.concatenate(arrays, axis=along)
    return tuple(jnp.split(lax.all_gather(both, axis, axis=dim, tiled=True), ends, axis=along))


def collected_together(shard, axis):
    leaves = jax.tree.leaves(shard)
    turns = sorted(range(len(leaves)), key=lambda k: -leaves[k].size)
    width = (1, *leaves[turns[0]].shape)[-1]
    lines = [
        jnp.pad(leaves[k].reshape(-1), (0, -leaves[k].size % width)).reshape(-1, width)
        for k in turns
    ]
    both, at, found = (lax.all_gather(jnp.concatenate(lines), axis), 0, {})
    for k, line in zip(turns, lines):
        share = both[:, at : at + len(line)].reshape(len(both), -1)
        found[k] = share[:, : leaves[k].size].reshape(-1, *leaves[k].shape)
        at += len(line)
    numbers = iter(range(len(leaves)))
    return jax.tree.map(lambda _: found[next(numbers)], shard)


def entering(shard, axis, combine, identity):
    size, index = (lax.axis_size(axis), lax.axis_index(axis))
    everything = collected_together(
        jax.tree.map(lambda part, kind: part.astype(kind), shard, (jnp.bfloat16, jnp.bfloat16)),
        axis,
    )
    start = jax.tree.map(
        lambda part, zero: jnp.broadcast_to(jnp.asarray(zero, part.dtype), part.shape),
        shard,
        identity,
    )

    def hop(k, before):
        reached = k < index
        new = combine(
            before, jax.tree.map(lambda part, own: part[k].astype(own.dtype), everything, shard)
        )
        return jax.tree.map(lambda a, b: jnp.where(reached, a, b), new, before)

    return lax.fori_loop(0, size, hop, start)


def in_blocks(shard, dim, size):
    before, after = (shard.shape[:dim], shard.shape[dim + 1 :])
    return jnp.moveaxis(shard.reshape(*before, size, -1, *after), dim, 0)


def summed_on_arrival(shard, axis, dim):
    size = lax.axis_size(axis)
    tiles = lax.all_to_all(in_blocks(shard, dim, size), axis, 0, 0, tiled=True)
    return jnp.sum(tiles.astype(jnp.float32), axis=0)


def head_norm(values, gain):
    square_mean = jnp.mean(values * values, axis=-1, keepdims=True)
    return values * lax.rsqrt(square_mean + epsilon) * gain


def recurrence_block(memory_matrix, inputs):
    query_slice, decay_part, key_slice, value_slice = inputs
    highest_score = lax.Precision.HIGHEST
    length = decay_part.shape[0]
    running_total = jnp.cumsum(decay_part, axis=0)
    causal = (
        lax.broadcasted_iota(jnp.int32, (length, length), 0)
        >= lax.broadcasted_iota(jnp.int32, (length, length), 1)
    )[:, :, None, None]
    relative = jnp.where(causal, running_total[:, None] - running_total[None, :], -jnp.inf)
    pairwise = jnp.sum(query_slice[:, None] * key_slice[None, :] * jnp.exp(relative), axis=-1)
    inner_part = jnp.einsum("tsh,shv->thv", pairwise, value_slice, precision=highest_score)
    carried_state = jnp.einsum(
        "fby,bym->fbm", query_slice * jnp.exp(running_total), memory_matrix, precision=highest_score
    )
    final_total = running_total[-1]
    updated_state = jnp.exp(final_total)[:, :, None] * memory_matrix + jnp.einsum(
        "rxc,rxa->xca",
        key_slice * jnp.exp(final_total[None] - running_total),
        value_slice,
        precision=highest_score,
    )
    return (updated_state, inner_part + carried_state)


def stick_piece(queries, shifts, weighted, keep_total, key_value, is_own, is_valid):
    scores = (
        jnp.einsum("thd,shd->hts", queries, key_value[0], preferred_element_type=jnp.float32)
        * HEAD ** (-0.5)
        + shifts[:, None, None]
    )
    logarithmic_retention = jax.nn.log_sigmoid(-scores)
    if is_own:
        rows_here = scores.shape[1]
        strict = lax.broadcasted_iota(jnp.int32, (rows_here, rows_here), 0) > lax.broadcasted_iota(
            jnp.int32, (rows_here, rows_here), 1
        )
        logarithmic_retention = jnp.where(strict, logarithmic_retention, 0.0)
    suffix = lax.cumsum(logarithmic_retention, axis=2, reverse=True) - logarithmic_retention
    log_weight = jax.nn.log_sigmoid(scores) + suffix + keep_total[:, :, None]
    if is_own:
        log_weight = jnp.where(strict, log_weight, -jnp.inf)
    weights = jnp.where(is_valid, jnp.exp(log_weight), 0.0).astype(jnp.bfloat16)
    weighted = weighted + jnp.einsum(
        "hts,shd->thd", weights, key_value[1], preferred_element_type=jnp.float32
    )
    keep_total = keep_total + jnp.where(is_valid, jnp.sum(logarithmic_retention, axis=2), 0.0)
    return (weighted, keep_total)


def contract_rows(rows_in, weight):
    return lax.dot_general(
        rows_in, weight, (((1,), (1,)), ((), ())), preferred_element_type=jnp.float32
    )


def on_device(
    input_layer_rows,
    input_norm_gain,
    query_weight_attention,
    key_weight_attention,
    value_weight_attention,
    query_weight_recurrent,
    forget_weight_recurrent,
    value_weight_recurrent,
    gate_weight_recurrent,
    output_weight_attention,
    emitted_projection_linear_scan,
    score_offset,
    attention_norm_gain,
    recurrence_norm_gain,
    forget_floor,
    forget_offset,
    extra_log_decay,
):
    values = input_layer_rows[0].astype(jnp.float32)
    square_mean = jnp.mean(values * values, axis=-1, keepdims=True)
    normed = (values * lax.rsqrt(square_mean + epsilon) * input_norm_gain).astype(jnp.bfloat16)
    tokens = normed.shape[0]
    weights_in = (
        query_weight_attention,
        key_weight_attention,
        value_weight_attention,
        query_weight_recurrent,
        forget_weight_recurrent,
        value_weight_recurrent,
        gate_weight_recurrent,
    )
    pieces = sent_together(
        (
            weights_in[0],
            weights_in[1],
            weights_in[2],
            weights_in[3],
            weights_in[4],
            weights_in[5],
            weights_in[6],
        ),
        ("sp", "fs"),
        0,
        1,
    )
    projected = tuple(
        (jnp.dot(normed, weight, preferred_element_type=jnp.float32) for weight in pieces)
    )
    query_a, key_a, value_a, query_b, forget_b, input_b, gate_b = [
        column_block.astype(jnp.bfloat16) for column_block in projected
    ]
    out_a, out_b = sent_together(
        (output_weight_attention, emitted_projection_linear_scan), ("sp", "fs"), 0, 1
    )
    head_count = query_a.shape[1] // HEAD
    queries = query_a.reshape(tokens, head_count, HEAD)
    key_value = jnp.stack(
        [key_a.reshape(tokens, head_count, HEAD), value_a.reshape(tokens, head_count, HEAD)]
    )
    weighted = jnp.zeros((tokens, head_count, HEAD), jnp.float32)
    keep_total = jnp.zeros((head_count, tokens), jnp.float32)
    weighted, keep_total = stick_piece(
        queries, score_offset, weighted, keep_total, key_value, True, True
    )
    position = lax.axis_index("sp")
    seq_devices = lax.axis_size("sp")
    gathered = lax.all_gather(key_value, "sp", axis=1, tiled=True)

    def gathered_turn(turn_index, carried_state):
        weighted_now, keep_now = carried_state
        source = jnp.maximum(position - turn_index, 0) * tokens
        piece_pair = lax.dynamic_slice_in_dim(gathered, source, tokens, 1)
        return stick_piece(
            queries, score_offset, weighted_now, keep_now, piece_pair, False, position >= turn_index
        )

    weighted, keep_total = lax.fori_loop(1, seq_devices, gathered_turn, (weighted, keep_total))
    row_log_total = jnp.log(jnp.maximum(-jnp.expm1(keep_total), log_floor))[None]
    mixed_a = (
        head_norm(weighted, attention_norm_gain.reshape(head_count, HEAD))
        .reshape(tokens, head_count * HEAD)
        .astype(jnp.bfloat16)
    )
    forget_logits = forget_b.astype(jnp.float32) + forget_offset
    forget_log_value = (
        jnp.logaddexp(
            jnp.log(forget_floor), jnp.log1p(-forget_floor) + jax.nn.log_sigmoid(forget_logits)
        )
        + extra_log_decay[0]
    )
    key_in = (1.0 - forget_floor) * jax.nn.sigmoid(-forget_logits)
    query_rows_input = jax.nn.silu(query_b.astype(jnp.float32)).reshape(tokens, head_count, HEAD)
    value_in = input_b.astype(jnp.float32)
    fading_channel_groups = forget_log_value.reshape(tokens, head_count, HEAD)
    shaped = tuple(
        (
            array_in.reshape(tokens // BLOCK, BLOCK, head_count, HEAD)
            for array_in in (query_rows_input, forget_log_value, key_in, value_in)
        )
    )
    empty_state = jnp.zeros((head_count, HEAD, HEAD), jnp.float32)
    nearby_hidden_vector, local_out = lax.scan(recurrence_block, empty_state, shaped)
    local_out = local_out.reshape(tokens, head_count, HEAD)
    through = jnp.exp(jnp.sum(fading_channel_groups, axis=0))

    def chain_states(earlier, later):
        return (earlier[0] * later[0], later[0][:, :, None] * earlier[1] + later[1])

    identity = (jnp.ones_like(through), jnp.zeros_like(nearby_hidden_vector))
    unused_decay, incoming_state = entering(
        (through, nearby_hidden_vector), "sp", chain_states, identity
    )
    running_sum = jnp.cumsum(fading_channel_groups, axis=0)
    recurrent = local_out + jnp.einsum(
        "fby,bym->fbm",
        query_rows_input * jnp.exp(running_sum),
        incoming_state,
        precision=lax.Precision.HIGHEST,
    )
    gated_out = head_norm(recurrent, recurrence_norm_gain.reshape(head_count, HEAD)) * jax.nn.silu(
        gate_b.astype(jnp.float32).reshape(tokens, head_count, HEAD)
    )
    mixed_b = gated_out.reshape(tokens, head_count * HEAD).astype(jnp.bfloat16)
    summed = summed_on_arrival(
        (contract_rows(mixed_a, out_a) + contract_rows(mixed_b, out_b)).astype(jnp.bfloat16),
        "tp",
        0,
    )
    layer_out = summed.astype(jnp.bfloat16)[None]
    return (layer_out, row_log_total)


def solution(mesh):
    return jax.shard_map(
        on_device,
        mesh=mesh,
        in_specs=(
            P("fs", "sp", None),
            P(),
            P(("sp", "fs"), "tp"),
            P(("sp", "fs"), "tp"),
            P(("sp", "fs"), "tp"),
            P(("sp", "fs"), "tp"),
            P(("sp", "fs"), "tp"),
            P(("sp", "fs"), "tp"),
            P(("sp", "fs"), "tp"),
            P(("sp", "fs"), "tp"),
            P(("sp", "fs"), "tp"),
            P("tp"),
            P("tp"),
            P("tp"),
            P("tp"),
            P("tp"),
            P("fs", "sp", "tp"),
        ),
        out_specs=(P("fs", ("sp", "tp"), None), P("fs", "tp", "sp")),
        check_vma=False,
    )
```

profile of v0, /device:TPU:1, one launch (start us, length us, event | category | flops | bytes accessed | tf_op | source)
XLA Modules:
  0.0 408.0 jit_solution(14859455435213965333)
XLA Ops:
  14.5 140.0 %all-gather.6.cloned.1.call-done = bf16[2048,896]{1,0:T(8,128)(2,1)} async-done(((bf16[32,896]{1,0:T(8,128)(2,1)}), bf16[2048,896]{1,0:T(8,128)(2,1)}) %all-gather.6.cloned.1.call-update) | async-done | bytes 3670032 | tf_op jit(solution)/shard_map/all_gather | solution.py:20
  165.0 8.8 %while.43 = (s32[]{:T(128)}, f32[1,128,128]{2,1,0:T(8,128)S(1)}, f32[4,64,1,128]{3,1,2,0:T(8,128)S(1)}, f32[4,64,1,128]{3,1,2,0:T(8,128)S(1)}, f32[4,64,1,128]{3...) while((s32[]{:T(128)}, f32[1,128,128]{2,1,0:T(8,128)S(1)}, ...), condition=%wide.region_13.14_spmd.clone, body=%wide.region_10.13_spmd.clone.sunk | while | flops 34693120 | bytes 962680 | solution.py:236
  173.8 27.1 %all-gather.1 = bf16[16,129,128]{2,1,0:T(8,128)(2,1)S(1)} all-gather(bf16[1,129,128]{2,1,0:T(8,128)(2,1)S(1)} %maximum_bitcast_fusion), channel_id=2, replica_groups=mesh['sp'=16,'fs'=4,'tp'=8] {'sp'}, dimensions={0}, use_global_device_ids=true | all-gather | bytes 561408 | tf_op jit(solution)/shard_map/all_gather | solution.py:31
  203.1 2.3 fusion.68
  208.6 18.3 %all-gather.8.cloned.1.call-done = bf16[2,4096,1,128]{3,1,2,0:T(8,128)(2,1)} async-done(((bf16[2,256,1,128]{3,1,2,0:T(8,128)(2,1)}), bf16[2,4096,1,128]{3,1,2,0:T(8,128)(2,1)}) %all-gather.8.cloned.1.call-update) | async-done | bytes 2097168 | tf_op jit(solution)/shard_map/all_gather | solution.py:201
  226.9 85.5 %while.42 = (s32[]{:T(128)}, f32[256,1,128]{0,2,1:T(8,128)S(1)}, f32[1,256]{1,0:T(1,128)S(1)}, s32[]{:T(128)}, bf16[2,4096,1,128]{3,1,2,0:T(8,128)(2,1)}, /*inde...) while((s32[]{:T(128)}, f32[256,1,128]{0,2,1:T(8,128)S(1)}, ...), condition=%wide.region_8.9_spmd, body=%wide.region_4.8_spmd.sunk | while | flops 43943176 | bytes 2841322 | solution.py:211
  228.7 2.3 fusion.141
  234.4 2.3 fusion.141
  240.1 2.3 fusion.141
  245.8 2.3 fusion.141
  251.5 2.3 fusion.141
  257.2 2.3 fusion.141
  262.9 2.3 fusion.141
  268.6 2.3 fusion.141
  274.3 2.3 fusion.141
  280.0 2.3 fusion.141
  285.7 2.3 fusion.141
  291.4 2.3 fusion.141
  297.1 2.3 fusion.141
  302.8 2.3 fusion.141
  312.4 53.6 %all-gather.10.cloned.1.call-done = bf16[2048,256]{1,0:T(8,128)(2,1)} async-done(((bf16[32,256]{1,0:T(8,128)(2,1)}), bf16[2048,256]{1,0:T(8,128)(2,1)}) %all-gather.10.cloned.1.call-update) | async-done | bytes 1048592 | tf_op jit(solution)/shard_map/all_gather | solution.py:20
  367.7 3.0 fusion.40
  370.7 15.0 %all-to-all-start = ((bf16[8,32,2048]{2,1,0:T(8,128)(2,1)}), bf16[8,32,2048]{2,1,0:T(8,128)(2,1)S(1)}, u32[]{:S(2)}, u32[]{:S(2)}) async-start(bf16[8,32,2048]{2,1,0:T(8,128)(2,1)} %bitcast.291), calls=%async_computation | async-start | bytes 2097152 | tf_op jit(solution)/shard_map/all_to_all | solution.py:69
  386.3 14.4 %all-to-all-done = bf16[8,32,2048]{2,1,0:T(8,128)(2,1)S(1)} async-done(((bf16[8,32,2048]{2,1,0:T(8,128)(2,1)}), bf16[8,32,2048]{2,1,0:T(8,128)(2,1)S(1)}, u32[]{:S(2)}, u32[]{:S(2)}) %all-to-all-start) | async-done | bytes 1048608 | tf_op jit(solution)/shard_map/all_to_all | solution.py:69
  (287 shorter events, 87.6 us)
Async XLA Ops:
  7.2 149.2 %copy-start = (bf16[1,256,2048]{2,1,0:T(8,128)(2,1)S(1)}, bf16[1,256,2048]{2,1,0:T(8,128)(2,1)}, u32[]{:S(2)}) copy-start(bf16[1,256,2048]{2,1,0:T(8,128)(2,1)} %param.23) | copy-start | bytes 3145732
  7.2 149.2 %copy-start.2 = (f32[2048]{0:T(1024)S(1)}, f32[2048]{0:T(1024)}, u32[]{:S(2)}) copy-start(f32[2048]{0:T(1024)} %param.24) | copy-start | bytes 24580
  7.2 147.3 %all-gather.6.cloned.1.call-start = ((), (), s32[]{:S(2)}) async-start(), calls=%async_computation.1 | async-start | bytes 3727360 | tf_op jit(solution)/shard_map/all_gather | solution.py:20
  12.2 0.6 copy-start.1
  12.9 214.0 %all-gather.8.cloned.1.call-start = ((), (), s32[]{:S(2)}) async-start(), calls=%async_computation.2 | async-start | bytes 2228224 | tf_op jit(solution)/shard_map/all_gather | solution.py:201
  156.4 2.3 copy-start.3
  156.4 2.3 copy-start.4
  156.4 3.0 copy-start.6
  158.6 207.4 %all-gather.10.cloned.1.call-start = ((), (), s32[]{:S(2)}) async-start(), calls=%async_computation.3 | async-start | bytes 1064960 | tf_op jit(solution)/shard_map/all_gather | solution.py:20
  161.6 1.6 copy-start.8
  161.6 1.6 copy-start.9
  226.9 139.2 %copy-start.7 = (f32[128]{0:T(128)S(1)}, f32[128]{0:T(128)}, u32[]{:S(2)}) copy-start(f32[128]{0:T(128)} %param.35) | copy-start | bytes 1540
  312.4 55.3 %copy-start.5 = (f32[128]{0:T(128)S(1)}, f32[128]{0:T(128)}, u32[]{:S(2)}) copy-start(f32[128]{0:T(128)} %param.36) | copy-start | bytes 1540
  370.7 30.0 %all-to-all-start = ((bf16[8,32,2048]{2,1,0:T(8,128)(2,1)}), bf16[8,32,2048]{2,1,0:T(8,128)(2,1)S(1)}, u32[]{:S(2)}, u32[]{:S(2)}) async-start(bf16[8,32,2048]{2,1,0:T(8,128)(2,1)} %bitcast.291), calls=%async_computation | async-start | bytes 2097152 | tf_op jit(solution)/shard_map/all_to_all | solution.py:69
Sparse Core Ops, SparseCore 0:
  13.0 141.4 all-gather.5
  158.8 68.0 all-gather.7
  229.8 136.2 all-gather.9
where the time goes:
time: 410 us; the launch traced here: 408 us
  waiting for transfers between devices  226 us (55%)
  matrix products  61.3 us (15%)
  other arithmetic  55.1 us (13%)
  blocking collectives  27.1 us (7%)
  starting transfers between devices  15.1 us (4%)
  between operations  14.7 us (4%)
  local copies, waits for them, and re-layouts  6.39 us (2%)
    all_gather x2, waiting for transfers between devices, sent_together(): lax.all_gather(both, axis, axis=dim, tiled=True)  194 us
    another operation x34, other arithmetic  37.4 us
    dot_general x16, matrix products, stick_piece(): jnp.einsum('thd,shd->hts', queries, key_value[0], preferred_element_type=...  28 us
    all_gather x1, blocking collectives, collected_together(): both, at, found = (lax.all_gather(jnp.concatenate(lines), axis), 0, {})  27.1 us
    all_gather x1, waiting for transfers between devices, on_device(): gathered = lax.all_gather(key_value, 'sp', axis=1, tiled=True)  18.3 us
    dot_general x16, matrix products, stick_piece(): jnp.einsum('hts,shd->thd', weights, key_value[1], preferred_element_type=...  15.9 us
    all_to_all x1, starting transfers between devices, summed_on_arrival(): tiles = lax.all_to_all(in_blocks(shard, dim, size), axis, 0, 0, tiled=True)  15 us
    all_to_all x1, waiting for transfers between devices, summed_on_arrival(): tiles = lax.all_to_all(in_blocks(shard, dim, size), axis, 0, 0, tiled=True)  14.4 us
  transfers between devices with their start and end apart: 4, of which 4 were waited for; matrix products, arithmetic and copies ran while one was open for 26% of the time, Pallas kernels for 0%

commit v1 on v0

v1 whole, which is shorter than its diff:
```python
import functools

import jax
import jax.numpy as jnp
from jax import lax
from jax.experimental import pallas as pl
from jax.experimental.pallas import tpu as pltpu
from jax.sharding import PartitionSpec as P

HEAD = 128
SUB = 16
EPS = 1e-06
FLOOR = 0.05
CHUNKS = 3
MESH = pl.DeviceIdType.MESH
F32 = jnp.float32
BF16 = jnp.bfloat16


def mm(a, b, ca=1, cb=0):
    return lax.dot_general(a, b, (((ca,), (cb,)), ((), ())), preferred_element_type=F32)


def split_mm(ones, a, terms):
    total = None
    for _ in range(terms):
        part = a.astype(BF16)
        a = a - part.astype(F32)
        term = mm(ones, part)
        total = term if total is None else total + term
    return total


def iotas(rows, cols):
    return (
        lax.broadcasted_iota(jnp.int32, (rows, cols), 0),
        lax.broadcasted_iota(jnp.int32, (rows, cols), 1),
    )


def sigmoid(v):
    return 1.0 / (1.0 + jnp.exp(-v))


def head_norm(v, gain):
    return v * lax.rsqrt(jnp.mean(v * v, axis=-1, keepdims=True) + EPS) * gain


def kernel(n, m, tp, *refs):
    (
        x_ref, gain_ref, qa_ref, ka_ref, va_ref, qb_ref, fb_ref, ib_ref, gb_ref, oa_ref, ob_ref,
        off_ref, again_ref, rgain_ref, floor_ref, foff_ref, extra_ref,
        out_ref, total_ref,
        xbuf, nbuf, ebuf, w0, w1, kvb, stb, qatt, accn, accf, keepn, keepf, incn, incf, decn, tri,
        qpad, rpad, kpad, vpad, recl, qdec, gate, mix, pbuf, prt, comb, xrecv,
        lsem, zus, zds, zur, zdr, yrs, yls, rrs, rls, lup, rdn, ldn, rup, l2, r2,
        bs, br, kus, kds, kur, kdr, ps, pr, xs, xr,
    ) = refs
    z, y, t8 = lax.axis_index("sp"), lax.axis_index("fs"), lax.axis_index("tp")
    tok, depth = xbuf.shape
    nup, ndn = n // 2, (n - 1) // 2
    half = n // 2
    zu, zd = lax.rem(z + 1, n), lax.rem(z + n - 1, n)
    yr, yl = lax.rem(y + 1, m), lax.rem(y + m - 1, m)
    nx = tp // 2
    core, xi = lax.rem(t8, 2), lax.div(t8, 2)
    partner = t8 + 1 - 2 * core

    local = [
        pltpu.make_async_copy(src, w0.at[z, y, :, pl.ds(k * HEAD, HEAD)], lsem.at[k])
        for k, src in enumerate((ka_ref, va_ref, qa_ref, fb_ref, ib_ref))
    ] + [
        pltpu.make_async_copy(src, w1.at[z, y, :, pl.ds(k * HEAD, HEAD)], lsem.at[5 + k])
        for k, src in enumerate((qb_ref, gb_ref, oa_ref, ob_ref))
    ]
    xcopy = pltpu.make_async_copy(x_ref.at[0], xbuf, lsem.at[9])
    ecopy = pltpu.make_async_copy(extra_ref.at[0], ebuf, lsem.at[10])
    for copy in local:
        copy.start()
    xcopy.start()
    ecopy.start()

    barrier = pltpu.get_barrier_semaphore()
    peers = [{"sp": zu}, {"sp": zd}]
    if m > 1:
        peers += [{"fs": yr}, {"fs": yl}]
    if tp > 1:
        peers += [{"tp": partner}]
        peers += [{"tp": lax.rem(xi + k, nx) * 2 + core} for k in range(1, nx)]
    for peer in peers:
        pl.semaphore_signal(barrier, inc=1, device_id=peer, device_id_type=MESH)
    for copy in local:
        copy.wait()
    pl.semaphore_wait(barrier, len(peers))

    def rc(src, dst, ssem, rsem, peer):
        return pltpu.make_async_remote_copy(
            src_ref=src, dst_ref=dst, send_sem=ssem, recv_sem=rsem, device_id=peer, device_id_type=MESH
        )

    ws = (w0, w1)

    def zup(g, t, block):
        ref = ws[g].at[block, y]
        return rc(ref, ref, zus.at[g], zur.at[g, t], {"sp": zu})

    def zdn(g, t, block):
        ref = ws[g].at[block, y]
        return rc(ref, ref, zds.at[g], zdr.at[g, t], {"sp": zd})

    def to_right(block, rsem):
        ref = w0.at[block, y]
        return rc(ref, ref, yrs, rsem, {"fs": yr})

    def to_left(block, rsem):
        ref = w0.at[block, y]
        return rc(ref, ref, yls, rsem, {"fs": yl})

    def relay_right(block):
        ref = w0.at[block, yl]
        return rc(ref, ref, rrs, l2, {"fs": yr})

    def relay_left(block):
        ref = w0.at[block, yr]
        return rc(ref, ref, rls, r2, {"fs": yl})

    def from_left(block, sem):
        ref = w0.at[block, yl]
        return rc(ref, ref, yrs, sem, {"fs": yr})

    def from_right(block, sem):
        ref = w0.at[block, yr]
        return rc(ref, ref, yls, sem, {"fs": yl})

    for g in (0, 1):
        zup(g, 0, z).start()
        if ndn:
            zdn(g, 0, z).start()
        if g == 0 and m > 1:
            to_right(z, lup.at[0]).start()
            to_left(z, rup).start()

    rows, cols = iotas(tok, tok)
    tri[...] = jnp.where(rows > cols, 1.0, 0.0).astype(BF16)
    xcopy.wait()

    @pl.loop(0, tok // 32)
    def _(r):
        at = pl.ds(pl.multiple_of(r * 32, 32), 32)
        v = xbuf[at, :].astype(F32)
        v = v * lax.rsqrt(jnp.mean(v * v, axis=-1, keepdims=True) + EPS)
        nbuf[at, :] = (v * gain_ref[...].reshape(1, depth)).astype(BF16)

    @pl.loop(1, nup + 1)
    def _(t):
        up, dn = lax.rem(z - t + n, n), lax.rem(z + t, n)
        zup(0, t - 1, up).wait_recv()

        @pl.when(t < nup)
        def _():
            zup(0, t, up).start()

        if m > 1:
            to_right(up, lup.at[t]).start()
            to_left(up, rup).start()

        if ndn:
            @pl.when(t <= ndn)
            def _():
                zdn(0, t - 1, dn).wait_recv()

                @pl.when(t < ndn)
                def _():
                    zdn(0, t, dn).start()

                if m > 1:
                    to_right(dn, ldn).start()
                    to_left(dn, rdn.at[t - 1]).start()

        zup(1, t - 1, up).wait_recv()

        @pl.when(t < nup)
        def _():
            zup(1, t, up).start()

        if ndn:
            @pl.when(t <= ndn)
            def _():
                zdn(1, t - 1, dn).wait_recv()

                @pl.when(t < ndn)
                def _():
                    zdn(1, t, dn).start()

        if m > 1:
            before = lax.rem(z - t + 1 + n, n)
            from_left(before, lup.at[t - 1]).wait_recv()
            relay_right(before).start()
            if ndn:
                @pl.when(t >= 2)
                def _():
                    late = lax.rem(z + t - 1, n)
                    from_right(late, rdn.at[t - 2]).wait_recv()
                    relay_left(late).start()

    last = lax.rem(z - nup + n, n)
    lo, hi = pl.ds(0, half), pl.ds(half, n - half)

    def bulk(k, part, src, peer):
        ref = w1.at[part, src]
        return rc(ref, ref, bs.at[k], br.at[k], peer)

    if m > 1:
        from_left(last, lup.at[nup]).wait_recv()
        relay_right(last).start()
        bulk(0, lo, y, {"fs": yr}).start()
        bulk(1, hi, y, {"fs": yl}).start()
        bulk(2, hi, y, {"fs": yr}).start()
        bulk(3, lo, y, {"fs": yl}).start()

        def waited(count, sem):
            ref = w0.at[pl.ds(0, count), 0]
            pltpu.make_async_copy(ref, ref, sem).wait()

        waited(nup + 1, rup)
        waited(nup + 1, l2)
        if ndn:
            waited(ndn, ldn)
            waited(ndn, r2)

    p0 = mm(nbuf[...], w0[...].reshape(depth, 5 * HEAD)).astype(BF16)
    kvb[z] = p0[:, : 2 * HEAD]
    qatt[...] = p0[:, 2 * HEAD : 3 * HEAD]
    floor = floor_ref[...].reshape(1, HEAD)
    u = p0[:, 3 * HEAD : 4 * HEAD].astype(F32) + foff_ref[...].reshape(1, HEAD)
    key = (1.0 - floor) * sigmoid(-u)
    ecopy.wait()
    step = jnp.log(1.0 - key) + ebuf[...]
    run = split_mm(jnp.where(rows >= cols, 1.0, 0.0).astype(BF16), step, 3)
    val = p0[:, 4 * HEAD : 5 * HEAD]
    end = run[tok - 1 :, :]
    state = mm(val, (key * jnp.exp(end - run)).astype(BF16), 0, 0)
    stb[z, :HEAD, :] = state.astype(BF16)
    stb[z, HEAD:, :] = jnp.broadcast_to(jnp.exp(end), (SUB, HEAD)).astype(BF16)
    zero = jnp.zeros((SUB, HEAD), F32)
    rpad[:SUB, :] = zero
    kpad[:SUB, :] = zero
    vpad[:SUB, :] = zero
    rpad[SUB:, :] = run
    kpad[SUB:, :] = key
    vpad[SUB:, :] = val.astype(F32)

    th = tok // 2

    def pieces(block):
        return (kvb.at[block, pl.ds(0, th)], kvb.at[block, pl.ds(th, th)], stb.at[block])

    def kup(t, block):
        return [
            rc(ref, ref, kus.at[t, c], kur.at[t, c], {"sp": zu}) for c, ref in enumerate(pieces(block))
        ]

    def kdn(t, block):
        return [
            rc(ref, ref, kds.at[t, c], kdr.at[t, c], {"sp": zd}) for c, ref in enumerate(pieces(block))
        ]

    @pl.when(z < n - 1)
    def _():
        for copy in kup(0, z):
            copy.start()

    if ndn:
        @pl.when(z < ndn)
        def _():
            for copy in kdn(0, z):
                copy.start()

    shift = off_ref[0]

    def attend(block, masked):
        s = mm(qatt[...], kvb[block, :, :HEAD], 1, 1) * HEAD ** (-0.5) + shift
        soft = jnp.maximum(s, 0.0) + jnp.log(1.0 + jnp.exp(-jnp.abs(s)))
        keep = -soft
        if masked:
            keep = jnp.where(rows > cols, keep, 0.0)
        big = keep.astype(BF16)
        small = (keep - big.astype(F32)).astype(BF16)
        suffix = mm(big, tri[...]) + mm(small, tri[...])
        w = jnp.exp(s - soft + suffix)
        if masked:
            w = jnp.where(rows > cols, w, 0.0)
        o = mm(w.astype(BF16), kvb[block, :, HEAD:])
        return o, jnp.broadcast_to(suffix[:, :1] + keep[:, :1], (tok, HEAD))

    o, gone = attend(z, True)
    accn[...] = o
    keepn[...] = gone
    accf[...] = jnp.zeros_like(accf)
    keepf[...] = jnp.zeros_like(keepf)
    incn[...] = jnp.zeros_like(incn)
    incf[...] = jnp.zeros_like(incf)
    decn[...] = jnp.ones_like(decn)

    def local_recurrence():
        pb = mm(nbuf[...], w1[:, :, :, : 2 * HEAD].reshape(depth, 2 * HEAD)).astype(BF16)
        q = pb[:, :HEAD].astype(F32)
        q = q * sigmoid(q)
        g = pb[:, HEAD:].astype(F32)
        gate[...] = g * sigmoid(g)
        r = rpad[SUB:, :]
        qdec[...] = (q * jnp.exp(r)).astype(BF16)
        ones = jnp.ones((HEAD, HEAD), BF16)
        place = lax.rem(lax.broadcasted_iota(jnp.int32, (tok, HEAD), 0), SUB)
        acc = jnp.zeros((tok, HEAD), F32)
        for d in range(SUB):
            at = pl.ds(SUB - d, tok)
            a = q * kpad[at, :] * jnp.exp(r - rpad[at, :])
            a = jnp.where(place >= d, a, 0.0)
            acc += mm(a.astype(BF16), ones) * vpad[at, :]
        recl[...] = acc
        qpad[...] = q
        for i in range(1, tok // SUB):
            b = i * SUB
            start = rpad[SUB + b - 1 : SUB + b, :]
            rt = rpad[SUB + b : 2 * SUB + b, :] - start
            top = jnp.maximum(jnp.max(rt, axis=0, keepdims=True), 0.0)
            qh = (qpad[b : b + SUB, :] * jnp.exp(rt - top)).astype(BF16)
            kh = kpad[SUB : SUB + b, :] * jnp.exp(start + top - rpad[SUB : SUB + b, :])
            pair = mm(qh, kh.astype(BF16), 1, 1).astype(BF16)
            recl[b : b + SUB, :] += mm(pair, vpad[SUB : SUB + b, :].astype(BF16))

    relay_at = min(3, max(nup - 1, 1))
    use_at = max(nup - 1, 1)

    @pl.loop(1, nup + 1)
    def _(t):
        up, dn = z - t, lax.rem(z + t, n)
        up0 = jnp.maximum(up, 0)
        for c in range(CHUNKS):
            @pl.when(z >= t)
            def _():
                kup(t - 1, up0)[c].wait_recv()

                @pl.when(jnp.logical_and(t < nup, z < n - 1))
                def _():
                    kup(t, up0)[c].start()

            if ndn:
                @pl.when(jnp.logical_and(t <= ndn, dn < ndn))
                def _():
                    kdn(t - 1, dn)[c].wait_recv()

                    @pl.when(t < ndn)
                    def _():
                        kdn(t, dn)[c].start()

        if m > 1:
            @pl.when(t == relay_at)
            def _():
                bulk(0, lo, yl, {"fs": yr}).wait_recv()
                bulk(4, lo, yl, {"fs": yr}).start()
                bulk(1, hi, yr, {"fs": yl}).wait_recv()
                bulk(5, hi, yr, {"fs": yl}).start()

        @pl.when(z >= t)
        def _():
            o, gone = attend(up0, False)
            accn[...] += jnp.exp(keepn[...]) * o
            keepn[...] += gone
            incn[...] += decn[:1, :] * stb[up0, :HEAD, :].astype(F32)
            decn[...] *= stb[up0, HEAD : HEAD + 8, :].astype(F32)

        if ndn:
            @pl.when(jnp.logical_and(t <= ndn, z + t >= n))
            def _():
                o, gone = attend(dn, False)
                accf[...] = o + jnp.exp(gone) * accf[...]
                keepf[...] += gone
                decay = stb[dn, HEAD : HEAD + 8, :].astype(F32)
                incf[...] = decay[:1, :] * incf[...] + stb[dn, :HEAD, :].astype(F32)

        @pl.when(t == use_at)
        def _():
            if m > 1:
                y2 = lax.rem(y + 2, m)
                bulk(2, hi, yl, {"fs": yr}).wait_recv()
                bulk(3, lo, yr, {"fs": yl}).wait_recv()
                bulk(4, lo, y2, {"fs": yr}).wait_recv()
                bulk(5, hi, y2, {"fs": yl}).wait_recv()
            local_recurrence()

    attended = accn[...] + jnp.exp(keepn[...]) * accf[...]
    keep = keepn[...] + keepf[...]
    logs = jnp.log(jnp.maximum(1.0 - jnp.exp(keep), FLOOR))
    total_ref[...] = jnp.transpose(logs)[:1, :].reshape(1, 1, tok)
    entering = incn[...] + decn[:1, :] * incf[...]
    recurrent = recl[...] + mm(qdec[...], entering.astype(BF16), 1, 1)
    mix[:, :HEAD] = head_norm(attended, again_ref[...].reshape(1, HEAD)).astype(BF16)
    mix[:, HEAD:] = (
        head_norm(recurrent, rgain_ref[...].reshape(1, HEAD)) * gate[...]
    ).astype(BF16)

    width = depth // 2

    def product(h):
        weight = w1[pl.ds(h * half, half), :, :, 2 * HEAD :].reshape(width, 2 * HEAD)
        return mm(mix[...], weight, 1, 1)

    if tp == 1:
        for h in range(2):
            out_ref[0, :, h * width : (h + 1) * width] = product(h).astype(BF16)
    else:
        def to_partner(h):
            return rc(pbuf.at[h, :, 1 - core], prt.at[h], ps.at[h], pr.at[h], {"tp": partner})

        def to_chip(h, k):
            x2 = lax.rem(xi + k, nx)
            return rc(
                comb.at[h, x2], xrecv.at[h, k - 1], xs.at[h, k - 1], xr.at[h, k - 1],
                {"tp": x2 * 2 + core},
            )

        for h in range(2):
            pbuf[h] = product(h).astype(BF16).reshape(nx, 2, tok // tp, width)
            to_partner(h).start()
        for h in range(2):
            to_partner(h).wait_recv()
            both = pbuf[h, :, core].astype(F32) + prt[h].astype(F32)
            comb[h] = both.astype(BF16)
            for k in range(1, nx):
                to_chip(h, k).start()
        for h in range(2):
            whole = comb[h, xi].astype(F32)
            for k in range(1, nx):
                to_chip(h, k).wait_recv()
                whole += xrecv[h, k - 1].astype(F32)
            out_ref[0, :, h * width : (h + 1) * width] = whole.astype(BF16)

    def sent(ref, sem):
        pltpu.make_async_copy(ref, ref, sem).wait()

    for g in (0, 1):
        sent(ws[g].at[pl.ds(0, nup), 0], zus.at[g])
        if ndn:
            sent(ws[g].at[pl.ds(0, ndn), 0], zds.at[g])
    if m > 1:
        sent(w0.at[pl.ds(0, n), 0], yrs)
        sent(w0.at[pl.ds(0, n), 0], yls)
        sent(w0.at[pl.ds(0, nup + 1), 0], rrs)
        if ndn:
            sent(w0.at[pl.ds(0, ndn), 0], rls)
        for k, part, peer in (
            (0, lo, yr), (1, hi, yl), (2, hi, yr), (3, lo, yl), (4, lo, yr), (5, hi, yl),
        ):
            bulk(k, part, y, {"fs": peer}).wait_send()

    @pl.loop(0, nup)
    def _(t):
        up, dn = jnp.maximum(z - t, 0), lax.rem(z + t, n)

        @pl.when(jnp.logical_and(z >= t, z < n - 1))
        def _():
            for copy in kup(t, up):
                copy.wait_send()

        if ndn:
            @pl.when(jnp.logical_and(t < ndn, dn < ndn))
            def _():
                for copy in kdn(t, dn):
                    copy.wait_send()

    if tp > 1:
        for h in range(2):
            to_partner(h).wait_send()
            for k in range(1, nx):
                to_chip(h, k).wait_send()


def on_device(n, m, tp, *args):
    tok, depth = args[0].shape[1:]
    nx = max(tp // 2, 1)
    rows = tok // tp
    nup, ndn = n // 2, max((n - 1) // 2, 1)
    vm, dma = pltpu.VMEM, pltpu.SemaphoreType.DMA
    whole = pl.BlockSpec(memory_space=pltpu.VMEM)
    there = pl.BlockSpec(memory_space=pl.ANY)
    scalar = pl.BlockSpec(memory_space=pltpu.SMEM)
    wide = (nx, 2, rows, depth // 2) if tp > 1 else (1, 1, 16, 128)
    part = (nx, rows, depth // 2) if tp > 1 else (1, 16, 128)
    return pl.pallas_call(
        functools.partial(kernel, n, m, tp),
        out_shape=(
            jax.ShapeDtypeStruct((1, rows, depth), BF16),
            jax.ShapeDtypeStruct((1, 1, tok), F32),
        ),
        in_specs=[there, whole] + [there] * 9 + [scalar] + [whole] * 4 + [there],
        out_specs=(whole, whole),
        scratch_shapes=[
            vm((tok, depth), BF16),
            vm((tok, depth), BF16),
            vm((tok, HEAD), F32),
            vm((n, m, 32, 5 * HEAD), BF16),
            vm((n, m, 32, 4 * HEAD), BF16),
            vm((n, tok, 2 * HEAD), BF16),
            vm((n, HEAD + SUB, HEAD), BF16),
            vm((tok, HEAD), BF16),
            vm((tok, HEAD), F32),
            vm((tok, HEAD), F32),
            vm((tok, HEAD), F32),
            vm((tok, HEAD), F32),
            vm((HEAD, HEAD), F32),
            vm((HEAD, HEAD), F32),
            vm((8, HEAD), F32),
            vm((tok, tok), BF16),
            vm((tok, HEAD), F32),
            vm((SUB + tok, HEAD), F32),
            vm((SUB + tok, HEAD), F32),
            vm((SUB + tok, HEAD), F32),
            vm((tok, HEAD), F32),
            vm((tok, HEAD), BF16),
            vm((tok, HEAD), F32),
            vm((tok, 2 * HEAD), BF16),
            vm((2, *wide), BF16),
            vm((2, *part), BF16),
            vm((2, *part), BF16),
            vm((2, max(nx - 1, 1), *part[1:]), BF16),
            dma((11,)),
            dma((2,)),
            dma((2,)),
            dma((2, nup)),
            dma((2, ndn)),
            dma,
            dma,
            dma,
            dma,
            dma((nup + 1,)),
            dma((ndn,)),
            dma,
            dma,
            dma,
            dma,
            dma((6,)),
            dma((6,)),
            dma((nup, CHUNKS)),
            dma((ndn, CHUNKS)),
            dma((nup, CHUNKS)),
            dma((ndn, CHUNKS)),
            dma((2,)),
            dma((2,)),
            dma((2, max(nx - 1, 1))),
            dma((2, max(nx - 1, 1))),
        ],
        compiler_params=pltpu.CompilerParams(
            collective_id=0, has_side_effects=True, vmem_limit_bytes=60 * 1024 * 1024
        ),
        name="layer",
    )(*args)


def solution(mesh):
    size = mesh.shape
    weight = P(("sp", "fs"), "tp")
    return jax.shard_map(
        functools.partial(on_device, size["sp"], size["fs"], size["tp"]),
        mesh=mesh,
        in_specs=(P("fs", "sp", None), P(), *[weight] * 9, *[P("tp")] * 5, P("fs", "sp", "tp")),
        out_specs=(P("fs", ("sp", "tp"), None), P("fs", "tp", "sp")),
        check_vma=False,
    )
```

time: 410 us -> 91.8 us (0.22)
  waiting for transfers between devices: 226 us -> 0 us
  Pallas kernels: 0 us -> 88.1 us
  matrix products: 61.3 us -> 0 us
  other arithmetic: 55.1 us -> 0 us
  blocking collectives: 27.1 us -> 0 us
  starting transfers between devices: 15.1 us -> 0 us
  between operations: 14.7 us -> 1.3 us
  local copies, waits for them, and re-layouts: 6.39 us -> 2.13 us
    all_gather x3 -> x0, waiting for transfers between devices: 212 us -> none  [the longest x2 194 us: sent_together(): lax.all_gather(both, axis, axis=dim, tiled=True)]
    pallas_call x0 -> x1, Pallas kernels: none -> 88.1 us  [on_device(): pl.pallas_call(functools.partial(kernel, n, m, tp), out_shape=(jax.ShapeD...]
    dot_general x53 -> x0, matrix products: 61.3 us -> none  [the longest x16 28 us: stick_piece(): jnp.einsum('thd,shd->hts', queries, key_value[0], preferred_element_type=...]
    another operation x39 -> x0, other arithmetic: 38.4 us -> none
    all_gather x1 -> x0, blocking collectives: 27.1 us -> none  [collected_together(): both, at, found = (lax.all_gather(jnp.concatenate(lines), axis), 0, {})]
    all_to_all x1 -> x0, starting transfers between devices: 15 us -> none  [summed_on_arrival(): tiles = lax.all_to_all(in_blocks(shard, dim, size), axis, 0, 0, tiled=True)]
    all_to_all x1 -> x0, waiting for transfers between devices: 14.4 us -> none  [summed_on_arrival(): tiles = lax.all_to_all(in_blocks(shard, dim, size), axis, 0, 0, tiled=True)]
    reduce_sum x7 -> x0, other arithmetic: 7.69 us -> none  [the longest x4 5.33 us: recurrence_block(): jnp.sum(query_slice[:, None] * key_slice[None, :] * jnp.exp(relative), ax...]
  transfers between devices with their start and end apart: 4 -> 0, of which waited for: 4 -> 0; matrix products, arithmetic and copies ran while one was open for 26% -> 0% of each run, Pallas kernels for 0% -> 0%
where the time goes in v1:
time: 91.8 us; the launch traced here: 91.6 us
  Pallas kernels  88.1 us (96%)
  local copies, waits for them, and re-layouts  2.13 us (2%)
  between operations  1.3 us (1%)
    pallas_call x1, Pallas kernels, on_device(): pl.pallas_call(functools.partial(kernel, n, m, tp), out_shape=(jax.ShapeD...  88.1 us
    unnamed x4, local copies, waits for them, and re-layouts  2.13 us

profile of v1, /device:TPU:1, one launch (start us, length us, event | category | flops | bytes accessed | tf_op | source)
XLA Modules:
  0.0 91.6 jit_solution(10346061280291512442)
XLA Ops:
  1.3 88.1 %layer.1 = (bf16[1,32,2048]{2,1,0:T(8,128)(2,1)}, f32[1,1,256]{2,1,0:T(1,128)}) custom-call(bf16[1,256,2048]{2,1,0:T(8,128)(2,1)} %refs_0_.1, f32[2048]{0:T(1024)} %refs_1_.1, bf16[32,128]{1,0:T(8,128)(2,1)} %refs_2_.1, bf16[32,128]{1,0:T(8,128)(2,1)} %refs_3_.1, bf16[32,128]{1,0:T(8,128)(2,1)} %refs_4_.1, bf16[32,128]{1,0:T(8,128)(2,1)} %refs_5_.1, ...), custom_call_target="tpu_custom_call" | custom-call | tf_op jit(solution)/shard_map/layer/pallas_call | solution.py:491
  89.4 0.0 copy-start
  89.4 1.6 %copy.22 = bf16[1,32,2048]{2,1,0:T(8,128)(2,1)} copy(bf16[1,32,2048]{2,1,0:T(8,128)(2,1)} %get-tuple-element.4) | data formatting | bytes 262144
  91.0 0.0 copy-done
  91.0 0.6 copy.23
Async XLA Ops:
  89.4 1.6 %copy-start = (f32[1,1,256]{2,1,0:T(1,128)S(1)}, f32[1,1,256]{2,1,0:T(1,128)}, u32[]{:S(2)}) copy-start(f32[1,1,256]{2,1,0:T(1,128)} %get-tuple-element.5) | copy-start | bytes 3076
